TPU v7x, 32 devices: a whole 2x2x4 slice. The times are simulated.
32 devices in a mesh: grp: 2 (over y), sp: 4 (over z), fs: 2 (over x), tp: 2 (over core).
Axes of the slice: x: 2, y: 2, z: 4, core: 2. Of those that a mesh axis runs over, the one named last changes fastest.
Arguments:
- tokens: bfloat16 [2, 6144, 2048], P('fs', ('grp', 'sp'), 'tp'), parts along dimension 1, may hold values from -12 to 12
- norm_gain: float32 [2048], replicated, may hold values from 0.1 to 1.9
- query_weight: bfloat16 [2048, 16, 64], P(None, 'tp'), may hold values from -3 to 3
- key_weight: bfloat16 [2048, 4, 64], P(None, 'tp'), may hold values from -3 to 3
- value_weight: bfloat16 [2048, 4, 64], P(None, 'tp'), may hold values from -0.125 to 0.125
- sink_logit: float32 [16], P('tp'), may hold values from 1 to 6
- pool_weight: bfloat16 [2048, 4, 256], P(None, None, 'tp'), may hold values from -0.125 to 0.125
- attn_out_weight: bfloat16 [16, 64, 2048], P('tp'), may hold values from -0.5 to 0.5
- pool_out_weight: bfloat16 [4, 256, 2048], P(None, 'tp'), may hold values from -0.1875 to 0.1875
Outputs:
- mixed: bfloat16 [2, 6144, 2048], P('fs', ('grp', 'sp', 'tp')), parts along dimension 1
There are 2 independent parts, one for each index of `grp`. A program takes and returns all parts, laid end to end along the dimension named above; an argument that names none is the same for every part. Nothing has to cross between parts.
All inputs are finite; a program needn't handle non-finite values.
Results may differ from a plain program's by a relative error of at most 0.0095.
The roundings to bfloat16 on the way count: a program that leaves them out, or rounds other values in their place, can miss the bound.
Values may be sent and summed in bfloat16 or wider, within the bound.
A program may use at most 128 MiB of HBM per device.

v0:
```python
import functools

import jax
import jax.numpy as jnp
from jax import lax
from jax.experimental import pallas as pl
from jax.experimental.pallas import tpu as pltpu
from jax.sharding import PartitionSpec as P

MESH = pl.DeviceIdType.MESH
WINDOW = 128
REACHES = (2, 4, 16)
TAIL = 16
CHUNK = 256
COLS = 512
F32 = jnp.float32
BF16 = jnp.bfloat16


def dot(a, b, dims=((1,), (0,))):
    return lax.dot_general(a, b, (dims, ((), ())), preferred_element_type=F32)


def kernel(
    n_sp,
    heads,
    local_kv,
    head_dim,
    tokens,
    gain,
    wq,
    wk,
    wv,
    sink,
    wp,
    wo,
    wpo,
    out,
    tok,
    normed,
    wqkv,
    wp_raw,
    wp_f32,
    wpool,
    wout,
    qt,
    kvt,
    ext,
    bands,
    block_sum,
    totals,
    act,
    sending,
    landing,
    w_sem,
    tok_sem,
    tok_send,
    tok_recv,
    halo_send,
    halo_recv,
    tot_send,
    tot_recv,
    out_send,
    out_recv,
    entered,
):
    me_sp = lax.axis_index("sp")
    me_tp = lax.axis_index("tp")
    other = 1 - me_tp
    rows, half_width = tokens.shape
    width = 2 * half_width
    q_rows = heads * head_dim
    kv_rows = local_kv * head_dim
    pool_cols = wpool.shape[1]
    channels = pool_cols // 4
    blocks = rows // WINDOW
    chunks = rows // CHUNK
    per_chunk = CHUNK // WINDOW
    half_rows = rows // 2
    half_blocks = blocks // 2
    tiles = width // COLS
    group = heads // local_kv

    for index in range(n_sp):
        totals[index] = jnp.zeros((8, channels), F32)
    barrier = pltpu.get_barrier_semaphore()
    pl.semaphore_signal(barrier, inc=1, device_id={"tp": other}, device_id_type=MESH)

    @pl.when(me_sp > 0)
    def _():
        pl.semaphore_signal(barrier, inc=1, device_id={"sp": me_sp - 1}, device_id_type=MESH)

    @pl.when(me_sp < n_sp - 1)
    def _():
        pl.semaphore_signal(barrier, inc=1, device_id={"sp": me_sp + 1}, device_id_type=MESH)

    load_wp = pltpu.make_async_copy(wp, wp_raw, w_sem.at[0])

    def local_tokens(c):
        at = pl.ds(pl.multiple_of(c * CHUNK, CHUNK), CHUNK)
        return pltpu.make_async_copy(tokens.at[at, :], tok.at[me_tp, at, :], tok_sem.at[c])

    def remote_tokens(c):
        at = pl.ds(pl.multiple_of(c * CHUNK, CHUNK), CHUNK)
        return pltpu.make_async_remote_copy(
            src_ref=tokens.at[at, :],
            dst_ref=tok.at[me_tp, at, :],
            send_sem=tok_send.at[c],
            recv_sem=tok_recv.at[c],
            device_id={"tp": other},
            device_id_type=MESH,
        )

    for c in reversed(range(chunks)):
        local_tokens(c).start()
    load_wp.start()
    loads = [
        pltpu.make_async_copy(wq, wqkv.at[pl.ds(0, q_rows), :], w_sem.at[1]),
        pltpu.make_async_copy(wk, wqkv.at[pl.ds(q_rows, kv_rows), :], w_sem.at[2]),
        pltpu.make_async_copy(wv, wqkv.at[pl.ds(q_rows + kv_rows, kv_rows), :], w_sem.at[3]),
    ]
    load_out = [
        pltpu.make_async_copy(wo, wout.at[pl.ds(0, q_rows), :], w_sem.at[4]),
        pltpu.make_async_copy(wpo, wout.at[pl.ds(q_rows, pool_cols), :], w_sem.at[5]),
    ]
    for load in loads:
        load.start()

    target = lax.broadcasted_iota(jnp.int32, (WINDOW, 2 * WINDOW), 0) + WINDOW
    source = lax.broadcasted_iota(jnp.int32, (WINDOW, 2 * WINDOW), 1)
    gap = target - source
    for g, reach in enumerate(REACHES):
        bands[g] = jnp.where((gap >= 0) & (gap < reach), 1.0, 0.0).astype(BF16)
    bands[3] = jnp.where((gap >= 0) & (gap < WINDOW) & (source >= WINDOW), 1.0, 0.0).astype(BF16)
    ext[pl.ds(0, WINDOW - TAIL), :] = jnp.zeros((WINDOW - TAIL, pool_cols), BF16)

    @pl.when(me_sp == 0)
    def _():
        ext[pl.ds(WINDOW - TAIL, TAIL), :] = jnp.zeros((TAIL, pool_cols), BF16)
        kvt[0] = jnp.zeros((2 * kv_rows, WINDOW), BF16)

    neighbours = jnp.where(me_sp > 0, 1, 0) + jnp.where(me_sp < n_sp - 1, 1, 0)
    pl.semaphore_wait(barrier, 1 + neighbours)
    for c in reversed(range(chunks)):
        remote_tokens(c).start()
    for load in load_out:
        load.start()

    load_wp.wait()
    part = wp_f32.shape[0]

    def regroup(i, carry):
        wp_f32[...] = wp_raw[pl.ds(pl.multiple_of(i * part, part), part), :].astype(F32)
        at = pl.ds(pl.multiple_of(i * (part // 4), part // 4), part // 4)
        for g in range(4):
            wpool[at, pl.ds(g * channels, channels)] = wp_f32[
                pl.ds(g, part // 4, stride=4), :
            ].astype(BF16)
        return carry

    lax.fori_loop(0, wp_raw.shape[0] // part, regroup, 0)
    for load in loads:
        load.wait()

    halo_kv = pltpu.make_async_remote_copy(
        src_ref=kvt.at[blocks],
        dst_ref=kvt.at[0],
        send_sem=halo_send.at[0],
        recv_sem=halo_recv.at[0],
        device_id={"sp": lax.rem(me_sp + 1, n_sp)},
        device_id_type=MESH,
    )
    halo_pool = pltpu.make_async_remote_copy(
        src_ref=ext.at[pl.ds(WINDOW + rows - TAIL, TAIL), :],
        dst_ref=ext.at[pl.ds(WINDOW - TAIL, TAIL), :],
        send_sem=halo_send.at[1],
        recv_sem=halo_recv.at[1],
        device_id={"sp": lax.rem(me_sp + 1, n_sp)},
        device_id_type=MESH,
    )

    scale = head_dim ** (-0.5)

    def normalize(c):
        local_tokens(c).wait()
        remote_tokens(c).wait_recv()
        at = pl.ds(pl.multiple_of(c * CHUNK, CHUNK), CHUNK)
        low = tok[0, at, :].astype(F32)
        high = tok[1, at, :].astype(F32)
        square = jnp.sum(low * low, axis=1, keepdims=True)
        square = square + jnp.sum(high * high, axis=1, keepdims=True)
        inv = lax.rsqrt(square * (1.0 / width) + 1e-06)
        normed[c, :, pl.ds(0, half_width)] = (low * inv * gain[:, pl.ds(0, half_width)]).astype(
            BF16
        )
        normed[c, :, pl.ds(half_width, half_width)] = (
            high * inv * gain[:, pl.ds(half_width, half_width)]
        ).astype(BF16)

    def project_pool(c):
        pooled_in = dot(normed[c], wpool[...]).astype(BF16)
        ext[pl.ds(pl.multiple_of(WINDOW + c * CHUNK, WINDOW), CHUNK), :] = pooled_in
        last = pooled_in[:, 3 * channels :].astype(F32)
        for j in range(per_chunk):
            summed = jnp.sum(last[j * WINDOW : (j + 1) * WINDOW], axis=0, keepdims=True)
            block_sum[c * per_chunk + j] = jnp.broadcast_to(summed, (8, channels))

    def project_qkv(c):
        qkv = dot(wqkv[...], normed[c], ((1,), (1,)))
        for j in range(per_chunk):
            b = c * per_chunk + j
            piece = qkv[:, j * WINDOW : (j + 1) * WINDOW]
            qt[b] = (piece[:q_rows] * scale).astype(BF16)
            kvt[b + 1] = piece[q_rows:].astype(BF16)

    def hear(step):
        @pl.when(me_sp + step < n_sp - 1)
        def _():
            pl.semaphore_wait(entered.at[step], 1)

    def tell(step):
        @pl.when((me_sp > 0) & (me_sp + step - 1 < n_sp - 1))
        def _():
            pl.semaphore_signal(
                entered.at[step], inc=1, device_id={"sp": me_sp - 1}, device_id_type=MESH
            )

    if n_sp > 2:
        tell(1)

    def project(i, carry):
        c = chunks - 1 - i
        normalize(c)

        @pl.when((i == 1) & (me_sp < n_sp - 1))
        def _():
            halo_kv.start()
            halo_pool.start()

        @pl.when(i > 0)
        def _():
            hear(i)
            tell(i + 1)

        project_pool(c)
        project_qkv(c)
        return carry

    lax.fori_loop(0, chunks, project, 0)

    for step in range(chunks, n_sp - 1):
        hear(step)
        if step < n_sp - 2:
            tell(step + 1)

    all_rows = block_sum[0]
    for b in range(1, blocks):
        all_rows = all_rows + block_sum[b]
    totals[me_sp] = all_rows

    def total_copy(step):
        return pltpu.make_async_remote_copy(
            src_ref=totals.at[me_sp],
            dst_ref=totals.at[me_sp],
            send_sem=tot_send.at[step],
            recv_sem=tot_recv.at[step],
            device_id={"sp": lax.rem(me_sp + step, n_sp)},
            device_id_type=MESH,
        )

    for step in range(1, n_sp):

        @pl.when(me_sp + step < n_sp)
        def _():
            total_copy(step).start()

    key_at = lax.broadcasted_iota(jnp.int32, (WINDOW, group * WINDOW), 0)
    query_at = lax.rem(
        lax.broadcasted_iota(jnp.int32, (WINDOW, group * WINDOW), 1), jnp.int32(WINDOW)
    )
    own_key = key_at <= query_at

    def attend(b, slot):
        bias = jnp.where((b == 0) & (me_sp == 0), -jnp.inf, 0.0).astype(F32)
        parts = []
        for h in range(local_kv):
            q = jnp.concatenate(
                [
                    qt[b, pl.ds((h * group + g) * head_dim, head_dim), :]
                    for g in range(group)
                ],
                axis=1,
            )
            s = jnp.concatenate(
                [jnp.full((1, WINDOW), sink[h * group + g], F32) for g in range(group)], axis=1
            )
            k_at = pl.ds(h * head_dim, head_dim)
            v_at = pl.ds(kv_rows + h * head_dim, head_dim)
            before = dot(kvt[b, k_at, :], q, ((0,), (0,))) + bias
            own = dot(kvt[b + 1, k_at, :], q, ((0,), (0,)))
            score = jnp.where(own_key, own, before)
            top = jnp.maximum(jnp.max(score, axis=0, keepdims=True), s)
            expo = jnp.exp(score - top)
            total = jnp.sum(expo, axis=0, keepdims=True) + jnp.exp(s - top)
            weight = expo * (1.0 / total)
            w_before = jnp.where(own_key, 0.0, weight).astype(BF16)
            w_own = jnp.where(own_key, weight, 0.0).astype(BF16)
            gathered = dot(kvt[b, v_at, :], w_before) + dot(kvt[b + 1, v_at, :], w_own)
            parts += [gathered[:, g * WINDOW : (g + 1) * WINDOW] for g in range(group)]
        attended = jnp.concatenate(parts, axis=0)
        act[pl.ds(pl.multiple_of(slot * WINDOW, WINDOW), WINDOW), pl.ds(0, q_rows)] = (
            attended.T.astype(BF16)
        )

    def pool(b, slot, carried):
        start = pl.multiple_of(b * WINDOW, WINDOW)
        position = me_sp * rows + b * WINDOW + 1
        count = (lax.broadcasted_iota(jnp.int32, (WINDOW, channels), 0) + position).astype(F32)
        at = pl.ds(pl.multiple_of(slot * WINDOW, WINDOW), WINDOW)
        for g in range(4):
            col = pl.ds(g * channels, channels)
            own = ext[pl.ds(start + WINDOW, WINDOW), col]
            if g < 3:
                sums = dot(bands[g], ext[pl.ds(start, 2 * WINDOW), col])
                denom = jnp.minimum(count, float(REACHES[g]))
            else:
                base = carried
                for earlier in range(blocks):
                    base = base + jnp.where(earlier < b, block_sum[earlier], 0.0)
                sums = dot(bands[3, :, pl.ds(WINDOW, WINDOW)], own) + base[:1]
                denom = count
            pooled = sums * (1.0 / denom) - own.astype(F32)
            act[at, pl.ds(q_rows + g * channels, channels)] = pooled.astype(BF16)

    @pl.when(me_sp > 0)
    def _():
        halo_kv.wait_recv()
        halo_pool.wait_recv()

    def attend_half(first):
        def one(i, carry):
            attend(first + i, i)
            return carry

        lax.fori_loop(0, half_blocks, one, 0, unroll=True)

    def pool_half(first, carried):
        def one(i, carry):
            pool(first + i, i, carried)
            return carry

        lax.fori_loop(0, half_blocks, one, 0, unroll=True)

    first = other * half_blocks
    attend_half(first)
    for step in range(1, n_sp):

        @pl.when(me_sp - step >= 0)
        def _():
            total_copy(step).wait_recv()

    carried = jnp.zeros((8, channels), F32)
    for index in range(n_sp):
        carried = carried + jnp.where(index < me_sp, totals[index], 0.0)
    pool_half(first, carried)
    for load in load_out:
        load.wait()

    def partial_send(t):
        return pltpu.make_async_remote_copy(
            src_ref=sending.at[t],
            dst_ref=landing.at[t],
            send_sem=out_send.at[t],
            recv_sem=out_recv.at[t],
            device_id={"tp": other},
            device_id_type=MESH,
        )

    def columns(t):
        return pl.ds(pl.multiple_of(t * COLS, COLS), COLS)

    def give(t, carry):
        sending[t] = dot(act[...], wout[:, columns(t)]).astype(BF16)
        partial_send(t).start()
        return carry

    lax.fori_loop(0, tiles, give, 0)

    first = me_tp * half_blocks
    attend_half(first)
    pool_half(first, carried)

    def keep(t, carry):
        partial_send(t).wait_recv()
        mine = dot(act[...], wout[:, columns(t)])
        out[:, columns(t)] = (mine + landing[t].astype(F32)).astype(BF16)
        return carry

    lax.fori_loop(0, tiles, keep, 0)
    for t in range(tiles):
        partial_send(t).wait_send()
    for c in range(chunks):
        remote_tokens(c).wait_send()
    for step in range(1, n_sp):

        @pl.when(me_sp + step < n_sp)
        def _():
            total_copy(step).wait_send()


    @pl.when(me_sp < n_sp - 1)
    def _():
        halo_kv.wait_send()
        halo_pool.wait_send()


def shards(n_sp, tokens, gain, wq, wk, wv, sink, wp, wo, wpo):
    rows, half_width = tokens.shape[1:]
    width = 2 * half_width
    heads, head_dim = wq.shape[1:]
    local_kv = wk.shape[1]
    channels = wp.shape[2]
    q_rows, kv_rows = (heads * head_dim, local_kv * head_dim)
    pool_cols = 4 * channels
    blocks = rows // WINDOW
    tiles = width // COLS
    chunks = rows // CHUNK
    dma = pltpu.SemaphoreType.DMA
    flat = lambda w: jnp.transpose(w, (1, 2, 0)).reshape(-1, width)
    hbm = pl.BlockSpec(memory_space=pltpu.HBM)
    vmem = pl.BlockSpec(memory_space=pltpu.VMEM)
    smem = pl.BlockSpec(memory_space=pltpu.SMEM)
    result = pl.pallas_call(
        functools.partial(kernel, n_sp, heads, local_kv, head_dim),
        out_shape=pltpu.VMEM((rows // 2, width), BF16),
        in_specs=[hbm, vmem, hbm, hbm, hbm, smem, hbm, hbm, hbm],
        out_specs=vmem,
        scratch_shapes=[
            pltpu.VMEM((2, rows, half_width), BF16),
            pltpu.VMEM((chunks, CHUNK, width), BF16),
            pltpu.VMEM((q_rows + 2 * kv_rows, width), BF16),
            pltpu.VMEM((4 * width, channels), BF16),
            pltpu.VMEM((1024, channels), F32),
            pltpu.VMEM((width, pool_cols), BF16),
            pltpu.VMEM((q_rows + pool_cols, width), BF16),
            pltpu.VMEM((blocks, q_rows, WINDOW), BF16),
            pltpu.VMEM((blocks + 1, 2 * kv_rows, WINDOW), BF16),
            pltpu.VMEM((rows + WINDOW, pool_cols), BF16),
            pltpu.VMEM((4, WINDOW, 2 * WINDOW), BF16),
            pltpu.VMEM((blocks, 8, channels), F32),
            pltpu.VMEM((n_sp, 8, channels), F32),
            pltpu.VMEM((rows // 2, q_rows + pool_cols), BF16),
            pltpu.VMEM((tiles, rows // 2, COLS), BF16),
            pltpu.VMEM((tiles, rows // 2, COLS), BF16),
            dma((6,)),
            dma((chunks,)),
            dma((chunks,)),
            dma((chunks,)),
            dma((2,)),
            dma((2,)),
            dma((n_sp,)),
            dma((n_sp,)),
            dma((tiles,)),
            dma((tiles,)),
            pltpu.SemaphoreType.REGULAR((n_sp,)),
        ],
        compiler_params=pltpu.CompilerParams(
            collective_id=0, has_side_effects=True, vmem_limit_bytes=67043328 - rows * width - 65536
        ),
    )(
        tokens[0],
        gain.reshape(1, width),
        flat(wq),
        flat(wk),
        flat(wv),
        sink,
        wp.reshape(-1, channels),
        wo.reshape(-1, width),
        wpo.reshape(-1, width),
    )
    return result[None]


def solution(mesh):
    in_specs = (
        P("fs", ("grp", "sp"), "tp"),
        P(),
        P(None, "tp", None),
        P(None, "tp", None),
        P(None, "tp", None),
        P("tp"),
        P(None, None, "tp"),
        P("tp", None, None),
        P(None, "tp", None),
    )
    out_specs = P("fs", ("grp", "sp", "tp"), None)
    return jax.shard_map(
        functools.partial(shards, mesh.shape["sp"]),
        mesh=mesh,
        in_specs=in_specs,
        out_specs=out_specs,
        check_vma=False,
    )
```

profile of v0, /device:TPU:1, one launch (start us, length us, event | category | flops | bytes accessed | tf_op | source)
XLA Modules:
  0.0 22.3 jit_solution(11835376838824834636)
XLA Ops:
  0.0 21.2 %shard_map.91 = bf16[384,2048]{1,0:T(8,128)(2,1)S(1)} custom-call(bf16[768,1024]{1,0:T(8,128)(2,1)} %bitcast.20, f32[1,2048]{1,0:T(1,128)} %bitcast.23, bf16[512,2048]{1,0:T(8,128)(2,1)} %bitcast.16, bf16[128,2048]{1,0:T(8,128)(2,1)} %bitcast.21, bf16[128,2048]{1,0:T(8,128)(2,1)} %bitcast.22, f32[8]{0:T(128)} %sink.1, bf16[8192,128]{1,0:T(8,128)(2,1)} %bitcast.17, ...), custom_call_target="tpu_custom_call" | custom-call | tf_op jit(solution)/shard_map/pallas_call | solution.py:433
  21.2 1.1 %copy.11 = bf16[1,384,2048]{2,1,0:T(8,128)(2,1)} copy(bf16[1,384,2048]{2,1,0:T(8,128)(2,1)S(1)} %bitcast.15) | data formatting | bytes 3145728
where the time goes:
time: 22.5 us; the launch traced here: 22.3 us
  Pallas kernels  21.2 us (94%)
  local copies, waits for them, and re-layouts  1.15 us (5%)
    pallas_call x1, Pallas kernels, shards(): pl.pallas_call(functools.partial(kernel, n_sp, heads, local_kv, head_dim)...  21.2 us
    unnamed x1, local copies, waits for them, and re-layouts  1.15 us

commit v1 on v0

--- a/solution.py
+++ b/solution.py
@@ -13,6 +13,7 @@
 TAIL = 16
 CHUNK = 256
 COLS = 512
+PAIR = 2
 F32 = jnp.float32
 BF16 = jnp.bfloat16
 
@@ -27,15 +28,18 @@
     local_kv,
     head_dim,
     tokens,
-    gain,
+    gain_hbm,
     wq,
     wk,
     wv,
-    sink,
+    sink_hbm,
     wp,
     wo,
     wpo,
     out,
+    gain,
+    sink,
+    tri,
     tok,
     normed,
     wqkv,
@@ -44,7 +48,8 @@
     wpool,
     wout,
     qt,
-    kvt,
+    keys,
+    vals,
     ext,
     bands,
     block_sum,
@@ -103,7 +108,7 @@
     def remote_tokens(c):
         at = pl.ds(pl.multiple_of(c * CHUNK, CHUNK), CHUNK)
         return pltpu.make_async_remote_copy(
-            src_ref=tokens.at[at, :],
+            src_ref=tok.at[me_tp, at, :],
             dst_ref=tok.at[me_tp, at, :],
             send_sem=tok_send.at[c],
             recv_sem=tok_recv.at[c],
@@ -111,9 +116,14 @@
             device_id_type=MESH,
         )
 
-    for c in reversed(range(chunks)):
+    load_gain = pltpu.make_async_copy(gain_hbm, gain, w_sem.at[6])
+    load_sink = pltpu.make_async_copy(sink_hbm, sink, w_sem.at[7])
+    local_tokens(chunks - 1).start()
+    load_wp.start()
+    for c in reversed(range(chunks - 1)):
         local_tokens(c).start()
-    load_wp.start()
+    load_gain.start()
+    load_sink.start()
     loads = [
         pltpu.make_async_copy(wq, wqkv.at[pl.ds(0, q_rows), :], w_sem.at[1]),
         pltpu.make_async_copy(wk, wqkv.at[pl.ds(q_rows, kv_rows), :], w_sem.at[2]),
@@ -131,22 +141,33 @@
     gap = target - source
     for g, reach in enumerate(REACHES):
         bands[g] = jnp.where((gap >= 0) & (gap < reach), 1.0, 0.0).astype(BF16)
+    tri[...] = jnp.where(
+        lax.broadcasted_iota(jnp.int32, (WINDOW, PAIR * WINDOW), 0)
+        <= lax.rem(lax.broadcasted_iota(jnp.int32, (WINDOW, PAIR * WINDOW), 1), jnp.int32(WINDOW)),
+        1.0,
+        0.0,
+    ).astype(BF16)
     bands[3] = jnp.where((gap >= 0) & (gap < WINDOW) & (source >= WINDOW), 1.0, 0.0).astype(BF16)
     ext[pl.ds(0, WINDOW - TAIL), :] = jnp.zeros((WINDOW - TAIL, pool_cols), BF16)
 
     @pl.when(me_sp == 0)
     def _():
         ext[pl.ds(WINDOW - TAIL, TAIL), :] = jnp.zeros((TAIL, pool_cols), BF16)
-        kvt[0] = jnp.zeros((2 * kv_rows, WINDOW), BF16)
+        keys[0] = jnp.zeros((WINDOW, kv_rows), BF16)
+        vals[0] = jnp.zeros((kv_rows, WINDOW), BF16)
 
     neighbours = jnp.where(me_sp > 0, 1, 0) + jnp.where(me_sp < n_sp - 1, 1, 0)
-    pl.semaphore_wait(barrier, 1 + neighbours)
-    for c in reversed(range(chunks)):
-        remote_tokens(c).start()
-    for load in load_out:
-        load.start()
-
-    load_wp.wait()
+    with jax.named_scope("barrier"):
+        pl.semaphore_wait(barrier, 1 + neighbours)
+    with jax.named_scope("send_tokens"):
+        for c in reversed(range(chunks)):
+            local_tokens(c).wait()
+            remote_tokens(c).start()
+        for load in load_out:
+            load.start()
+
+    with jax.named_scope("wait_wp"):
+        load_wp.wait()
     part = wp_f32.shape[0]
 
     def regroup(i, carry):
@@ -158,18 +179,26 @@
             ].astype(BF16)
         return carry
 
-    lax.fori_loop(0, wp_raw.shape[0] // part, regroup, 0)
-    for load in loads:
-        load.wait()
-
-    halo_kv = pltpu.make_async_remote_copy(
-        src_ref=kvt.at[blocks],
-        dst_ref=kvt.at[0],
-        send_sem=halo_send.at[0],
-        recv_sem=halo_recv.at[0],
-        device_id={"sp": lax.rem(me_sp + 1, n_sp)},
-        device_id_type=MESH,
-    )
+    with jax.named_scope("regroup"):
+        lax.fori_loop(0, wp_raw.shape[0] // part, regroup, 0)
+    with jax.named_scope("wait_wqkv"):
+        for load in loads:
+            load.wait()
+        load_gain.wait()
+        load_sink.wait()
+
+    def halo_copy(buffer, index):
+        return pltpu.make_async_remote_copy(
+            src_ref=buffer.at[blocks],
+            dst_ref=buffer.at[0],
+            send_sem=halo_send.at[index],
+            recv_sem=halo_recv.at[index],
+            device_id={"sp": lax.rem(me_sp + 1, n_sp)},
+            device_id_type=MESH,
+        )
+
+    halo_keys = halo_copy(keys, 0)
+    halo_vals = halo_copy(vals, 2)
     halo_pool = pltpu.make_async_remote_copy(
         src_ref=ext.at[pl.ds(WINDOW + rows - TAIL, TAIL), :],
         dst_ref=ext.at[pl.ds(WINDOW - TAIL, TAIL), :],
@@ -182,8 +211,8 @@
     scale = head_dim ** (-0.5)
 
     def normalize(c):
-        local_tokens(c).wait()
-        remote_tokens(c).wait_recv()
+        with jax.named_scope("wait_tokens"):
+            remote_tokens(c).wait_recv()
         at = pl.ds(pl.multiple_of(c * CHUNK, CHUNK), CHUNK)
         low = tok[0, at, :].astype(F32)
         high = tok[1, at, :].astype(F32)
@@ -211,7 +240,8 @@
             b = c * per_chunk + j
             piece = qkv[:, j * WINDOW : (j + 1) * WINDOW]
             qt[b] = (piece[:q_rows] * scale).astype(BF16)
-            kvt[b + 1] = piece[q_rows:].astype(BF16)
+            keys[b + 1] = piece[q_rows : q_rows + kv_rows].T.astype(BF16)
+            vals[b + 1] = piece[q_rows + kv_rows :].astype(BF16)
 
     def hear(step):
         @pl.when(me_sp + step < n_sp - 1)
@@ -230,11 +260,13 @@
 
     def project(i, carry):
         c = chunks - 1 - i
-        normalize(c)
+        with jax.named_scope("normalize"):
+            normalize(c)
 
         @pl.when((i == 1) & (me_sp < n_sp - 1))
         def _():
-            halo_kv.start()
+            halo_keys.start()
+            halo_vals.start()
             halo_pool.start()
 
         @pl.when(i > 0)
@@ -242,8 +274,9 @@
             hear(i)
             tell(i + 1)
 
-        project_pool(c)
-        project_qkv(c)
+        with jax.named_scope("project"):
+            project_pool(c)
+            project_qkv(c)
         return carry
 
     lax.fori_loop(0, chunks, project, 0)
@@ -274,43 +307,75 @@
         def _():
             total_copy(step).start()
 
-    key_at = lax.broadcasted_iota(jnp.int32, (WINDOW, group * WINDOW), 0)
-    query_at = lax.rem(
-        lax.broadcasted_iota(jnp.int32, (WINDOW, group * WINDOW), 1), jnp.int32(WINDOW)
+    own_key = lax.broadcasted_iota(jnp.int32, (WINDOW, PAIR * WINDOW), 0) <= lax.rem(
+        lax.broadcasted_iota(jnp.int32, (WINDOW, PAIR * WINDOW), 1), jnp.int32(WINDOW)
     )
-    own_key = key_at <= query_at
-
-    def attend(b, slot):
-        bias = jnp.where((b == 0) & (me_sp == 0), -jnp.inf, 0.0).astype(F32)
-        parts = []
-        for h in range(local_kv):
-            q = jnp.concatenate(
-                [
-                    qt[b, pl.ds((h * group + g) * head_dim, head_dim), :]
-                    for g in range(group)
-                ],
-                axis=1,
-            )
-            s = jnp.concatenate(
-                [jnp.full((1, WINDOW), sink[h * group + g], F32) for g in range(group)], axis=1
-            )
-            k_at = pl.ds(h * head_dim, head_dim)
-            v_at = pl.ds(kv_rows + h * head_dim, head_dim)
-            before = dot(kvt[b, k_at, :], q, ((0,), (0,))) + bias
-            own = dot(kvt[b + 1, k_at, :], q, ((0,), (0,)))
-            score = jnp.where(own_key, own, before)
-            top = jnp.maximum(jnp.max(score, axis=0, keepdims=True), s)
-            expo = jnp.exp(score - top)
-            total = jnp.sum(expo, axis=0, keepdims=True) + jnp.exp(s - top)
-            weight = expo * (1.0 / total)
-            w_before = jnp.where(own_key, 0.0, weight).astype(BF16)
-            w_own = jnp.where(own_key, weight, 0.0).astype(BF16)
-            gathered = dot(kvt[b, v_at, :], w_before) + dot(kvt[b + 1, v_at, :], w_own)
-            parts += [gathered[:, g * WINDOW : (g + 1) * WINDOW] for g in range(group)]
-        attended = jnp.concatenate(parts, axis=0)
-        act[pl.ds(pl.multiple_of(slot * WINDOW, WINDOW), WINDOW), pl.ds(0, q_rows)] = (
-            attended.T.astype(BF16)
-        )
+    none = jnp.zeros((head_dim, PAIR * WINDOW), BF16)
+
+    def unit_scores(unit):
+        b, slot, h, p, edge = unit
+        first_head = h * group + p * PAIR
+        q = jnp.concatenate(
+            [
+                qt[b, pl.ds((first_head + g) * head_dim, head_dim), :]
+                for g in range(PAIR)
+            ],
+            axis=1,
+        )
+        rhs = jnp.concatenate([q if k == h else none for k in range(local_kv)], axis=0)
+        before = dot(keys[b], rhs)
+        own = dot(keys[b + 1], rhs)
+        return before, own
+
+    def unit_weights(unit, scores):
+        b, slot, h, p, edge = unit
+        first_head = h * group + p * PAIR
+        before, own = scores
+        if edge:
+            before = before + jnp.where((b == 0) & (me_sp == 0), -jnp.inf, 0.0).astype(F32)
+        s = jnp.concatenate(
+            [jnp.full((1, WINDOW), sink[first_head + g], F32) for g in range(PAIR)], axis=1
+        )
+        score = jnp.where(own_key, own, before)
+        top = jnp.maximum(jnp.max(score, axis=0, keepdims=True), s)
+        expo = jnp.exp(score - top)
+        total = jnp.sum(expo, axis=0, keepdims=True) + jnp.exp(s - top)
+        weight = (expo * (1.0 / total)).astype(BF16)
+        w_own = weight * tri[...]
+        return jnp.concatenate([weight - w_own, w_own], axis=0)
+
+    def unit_output(unit, weights):
+        b, slot, h, p, edge = unit
+        first_head = h * group + p * PAIR
+        v_at = pl.ds(h * head_dim, head_dim)
+        v = jnp.concatenate([vals[b, v_at, :], vals[b + 1, v_at, :]], axis=1)
+        gathered = dot(v, weights)
+        stacked = jnp.concatenate(
+            [gathered[:, g * WINDOW : (g + 1) * WINDOW] for g in range(PAIR)], axis=0
+        )
+        act[pl.ds(slot * WINDOW, WINDOW), pl.ds(first_head * head_dim, PAIR * head_dim)] = (
+            stacked.T.astype(BF16)
+        )
+
+    def attend(units, fillers=()):
+        scores, weights = {}, {}
+        for step in range(len(units) + 2):
+            if step < len(units):
+                scores[step] = unit_scores(units[step])
+            if step < len(fillers):
+                fillers[step]()
+            if 0 <= step - 1 < len(units):
+                weights[step - 1] = unit_weights(units[step - 1], scores.pop(step - 1))
+            if 0 <= step - 2:
+                unit_output(units[step - 2], weights.pop(step - 2))
+
+    def units_of(first):
+        return [
+            (first + i, i, h, p, i == 0)
+            for i in range(half_blocks)
+            for h in range(local_kv)
+            for p in range(group // PAIR)
+        ]
 
     def pool(b, slot, carried):
         start = pl.multiple_of(b * WINDOW, WINDOW)
@@ -332,17 +397,12 @@
             pooled = sums * (1.0 / denom) - own.astype(F32)
             act[at, pl.ds(q_rows + g * channels, channels)] = pooled.astype(BF16)
 
-    @pl.when(me_sp > 0)
-    def _():
-        halo_kv.wait_recv()
-        halo_pool.wait_recv()
-
-    def attend_half(first):
-        def one(i, carry):
-            attend(first + i, i)
-            return carry
-
-        lax.fori_loop(0, half_blocks, one, 0, unroll=True)
+    with jax.named_scope("wait_halo"):
+        @pl.when(me_sp > 0)
+        def _():
+            halo_keys.wait_recv()
+            halo_vals.wait_recv()
+            halo_pool.wait_recv()
 
     def pool_half(first, carried):
         def one(i, carry):
@@ -352,17 +412,20 @@
         lax.fori_loop(0, half_blocks, one, 0, unroll=True)
 
     first = other * half_blocks
-    attend_half(first)
-    for step in range(1, n_sp):
-
-        @pl.when(me_sp - step >= 0)
-        def _():
-            total_copy(step).wait_recv()
+    with jax.named_scope("attend1"):
+        attend(units_of(first))
+    with jax.named_scope("wait_totals"):
+        for step in range(1, n_sp):
+
+            @pl.when(me_sp - step >= 0)
+            def _():
+                total_copy(step).wait_recv()
 
     carried = jnp.zeros((8, channels), F32)
     for index in range(n_sp):
         carried = carried + jnp.where(index < me_sp, totals[index], 0.0)
-    pool_half(first, carried)
+    with jax.named_scope("pool1"):
+        pool_half(first, carried)
     for load in load_out:
         load.wait()
 
@@ -379,24 +442,29 @@
     def columns(t):
         return pl.ds(pl.multiple_of(t * COLS, COLS), COLS)
 
-    def give(t, carry):
+    def give(t):
         sending[t] = dot(act[...], wout[:, columns(t)]).astype(BF16)
-        partial_send(t).start()
-        return carry
-
-    lax.fori_loop(0, tiles, give, 0)
+
+    with jax.named_scope("give"):
+        for t in range(0, tiles, 2):
+            give(t)
+            give(t + 1)
+            partial_send(t).start()
+            partial_send(t + 1).start()
 
     first = me_tp * half_blocks
-    attend_half(first)
-    pool_half(first, carried)
-
-    def keep(t, carry):
-        partial_send(t).wait_recv()
-        mine = dot(act[...], wout[:, columns(t)])
-        out[:, columns(t)] = (mine + landing[t].astype(F32)).astype(BF16)
-        return carry
-
-    lax.fori_loop(0, tiles, keep, 0)
+    with jax.named_scope("attend2"):
+        attend(units_of(first))
+    with jax.named_scope("pool2"):
+        pool_half(first, carried)
+
+    with jax.named_scope("wait_give"):
+        for t in range(tiles):
+            partial_send(t).wait_recv()
+    with jax.named_scope("keep"):
+        for t in range(tiles):
+            mine = dot(act[...], wout[:, columns(t)])
+            out[:, columns(t)] = (mine + landing[t].astype(F32)).astype(BF16)
     for t in range(tiles):
         partial_send(t).wait_send()
     for c in range(chunks):
@@ -410,7 +478,8 @@
 
     @pl.when(me_sp < n_sp - 1)
     def _():
-        halo_kv.wait_send()
+        halo_keys.wait_send()
+        halo_vals.wait_send()
         halo_pool.wait_send()
 
 
@@ -429,13 +498,15 @@
     flat = lambda w: jnp.transpose(w, (1, 2, 0)).reshape(-1, width)
     hbm = pl.BlockSpec(memory_space=pltpu.HBM)
     vmem = pl.BlockSpec(memory_space=pltpu.VMEM)
-    smem = pl.BlockSpec(memory_space=pltpu.SMEM)
     result = pl.pallas_call(
         functools.partial(kernel, n_sp, heads, local_kv, head_dim),
         out_shape=pltpu.VMEM((rows // 2, width), BF16),
-        in_specs=[hbm, vmem, hbm, hbm, hbm, smem, hbm, hbm, hbm],
+        in_specs=[hbm] * 9,
         out_specs=vmem,
         scratch_shapes=[
+            pltpu.VMEM((1, width), F32),
+            pltpu.SMEM((heads,), F32),
+            pltpu.VMEM((WINDOW, PAIR * WINDOW), BF16),
             pltpu.VMEM((2, rows, half_width), BF16),
             pltpu.VMEM((chunks, CHUNK, width), BF16),
             pltpu.VMEM((q_rows + 2 * kv_rows, width), BF16),
@@ -444,7 +515,8 @@
             pltpu.VMEM((width, pool_cols), BF16),
             pltpu.VMEM((q_rows + pool_cols, width), BF16),
             pltpu.VMEM((blocks, q_rows, WINDOW), BF16),
-            pltpu.VMEM((blocks + 1, 2 * kv_rows, WINDOW), BF16),
+            pltpu.VMEM((blocks + 1, WINDOW, kv_rows), BF16),
+            pltpu.VMEM((blocks + 1, kv_rows, WINDOW), BF16),
             pltpu.VMEM((rows + WINDOW, pool_cols), BF16),
             pltpu.VMEM((4, WINDOW, 2 * WINDOW), BF16),
             pltpu.VMEM((blocks, 8, channels), F32),
@@ -452,12 +524,12 @@
             pltpu.VMEM((rows // 2, q_rows + pool_cols), BF16),
             pltpu.VMEM((tiles, rows // 2, COLS), BF16),
             pltpu.VMEM((tiles, rows // 2, COLS), BF16),
-            dma((6,)),
+            dma((8,)),
             dma((chunks,)),
             dma((chunks,)),
             dma((chunks,)),
-            dma((2,)),
-            dma((2,)),
+            dma((3,)),
+            dma((3,)),
             dma((n_sp,)),
             dma((n_sp,)),
             dma((tiles,)),

time: 22.5 us -> 20.1 us (0.89)
  the two profiles are of different devices: /device:TPU:1 before, /device:TPU:0 now
where the time goes in v1:
time: 20.1 us; the launch traced here: 20 us
  Pallas kernels  18.8 us (94%)
  local copies, waits for them, and re-layouts  1.15 us (6%)
    pallas_call x1, Pallas kernels, shards(): pl.pallas_call(functools.partial(kernel, n_sp, heads, local_kv, head_dim)...  18.8 us
    unnamed x1, local copies, waits for them, and re-layouts  1.15 us

profile of v1, /device:TPU:0, one launch (start us, length us, event | category | flops | bytes accessed | tf_op | source)
XLA Modules:
  0.0 20.0 jit_solution(13675738688078262645)
XLA Ops:
  0.0 18.8 %shard_map.91 = bf16[384,2048]{1,0:T(8,128)(2,1)S(1)} custom-call(bf16[768,1024]{1,0:T(8,128)(2,1)} %bitcast.20, f32[1,2048]{1,0:T(1,128)} %bitcast.23, bf16[512,2048]{1,0:T(8,128)(2,1)} %bitcast.16, bf16[128,2048]{1,0:T(8,128)(2,1)} %bitcast.21, bf16[128,2048]{1,0:T(8,128)(2,1)} %bitcast.22, f32[8]{0:T(128)} %sink_hbm.1, bf16[8192,128]{1,0:T(8,128)(2,1)} %bitcast.17, ...), custom_call_target="tpu_custom_call" | custom-call | tf_op jit(solution)/shard_map/pallas_call | solution.py:501
  18.8 1.1 %copy.11 = bf16[1,384,2048]{2,1,0:T(8,128)(2,1)} copy(bf16[1,384,2048]{2,1,0:T(8,128)(2,1)S(1)} %bitcast.15) | data formatting | bytes 3145728

commit v2 on v1

v2 whole, which is shorter than its diff:
```python
import functools

import jax
import jax.numpy as jnp
from jax import lax
from jax.experimental import pallas as pl
from jax.experimental.pallas import tpu as pltpu
from jax.sharding import PartitionSpec as P

MESH = pl.DeviceIdType.MESH
WINDOW = 128
REACHES = (2, 4, 16)
TAIL = 16
CHUNK = 256
COLS = 512
PAIR = 2
F32 = jnp.float32
BF16 = jnp.bfloat16
scope = jax.named_scope


def dot(a, b, dims=((1,), (0,))):
    return lax.dot_general(a, b, (dims, ((), ())), preferred_element_type=F32)


def normalize(low_ref, high_ref, gain, store):
    half_width = low_ref.shape[1]
    low = low_ref[...].astype(F32)
    high = high_ref[...].astype(F32)
    square = jnp.sum(low * low, axis=1, keepdims=True)
    square = square + jnp.sum(high * high, axis=1, keepdims=True)
    inv = lax.rsqrt(square * (0.5 / half_width) + 1e-06)
    low_at, high_at = pl.ds(0, half_width), pl.ds(half_width, half_width)
    store(low_at, (low * inv * gain[:, low_at]).astype(BF16))
    store(high_at, (high * inv * gain[:, high_at]).astype(BF16))


def store_into(ref):
    def store(at, value):
        ref[:, at] = value

    return store


def project_pool(normed, wpool, ext_rows, sums):
    pooled_in = dot(normed[...], wpool[...]).astype(BF16)
    ext_rows[...] = pooled_in
    channels = pooled_in.shape[1] // 4
    last = pooled_in[:, 3 * channels :].astype(F32)
    for j in range(pooled_in.shape[0] // WINDOW):
        summed = jnp.sum(last[j * WINDOW : (j + 1) * WINDOW], axis=0, keepdims=True)
        sums[j] = jnp.broadcast_to(summed, (8, channels))


def mix_kernel(
    n_sp,
    heads,
    local_kv,
    head_dim,
    tokens,
    gain_hbm,
    wq,
    wk,
    wv,
    wp,
    wo,
    wpo,
    sink_hbm,
    act,
    out_left,
    landing_right,
    wout,
    tok,
    normed,
    gain,
    sink,
    wp_raw,
    wp_f32,
    wpool,
    wqkv,
    tri,
    bands,
    qt,
    keys,
    vals,
    ext,
    block_sum,
    totals,
    sending,
    landing_left,
    w_sem,
    tok_sem,
    tok_send,
    tok_recv,
    halo_send,
    halo_recv,
    tot_send,
    tot_recv,
    out_send,
    out_recv,
    ready,
):
    me_sp = lax.axis_index("sp")
    me_tp = lax.axis_index("tp")
    other = 1 - me_tp
    width = wout.shape[1]
    q_rows = heads * head_dim
    kv_rows = local_kv * head_dim
    pool_cols = wpool.shape[1]
    channels = pool_cols // 4
    rows = act.shape[0]
    blocks = rows // WINDOW
    chunks = rows // CHUNK
    per_chunk = CHUNK // WINDOW
    half_rows = rows // 2
    half_blocks = blocks // 2
    tiles = width // COLS
    left_tiles = landing_left.shape[0]
    group = heads // local_kv

    def either(for_zero, for_one):
        return for_zero + me_tp * (for_one - for_zero)

    for index in range(n_sp):
        totals[index] = jnp.zeros((8, channels), F32)
    barrier = pltpu.get_barrier_semaphore()

    @pl.when(me_tp == 1)
    def _():
        pl.semaphore_signal(barrier, inc=1, device_id={"tp": 0}, device_id_type=MESH)

    def local_tokens(c):
        return pltpu.make_async_copy(
            tokens.at[pl.ds(c * CHUNK, CHUNK), :], tok.at[c, me_tp], tok_sem.at[c]
        )

    def remote_tokens(c):
        direct = c == chunks - 1
        return pltpu.make_async_remote_copy(
            src_ref=tokens.at[pl.ds(c * CHUNK, CHUNK), :] if direct else tok.at[c, me_tp],
            dst_ref=tok.at[c, me_tp],
            send_sem=tok_send.at[c],
            recv_sem=tok_recv.at[c],
            device_id={"tp": other},
            device_id_type=MESH,
        )

    load_wp = pltpu.make_async_copy(wp, wp_raw, w_sem.at[0])
    load_gain = pltpu.make_async_copy(gain_hbm, gain, w_sem.at[1])
    loads = [
        pltpu.make_async_copy(wq, wqkv.at[pl.ds(0, q_rows), :], w_sem.at[2]),
        pltpu.make_async_copy(wk, wqkv.at[pl.ds(q_rows, kv_rows), :], w_sem.at[3]),
        pltpu.make_async_copy(wv, wqkv.at[pl.ds(q_rows + kv_rows, kv_rows), :], w_sem.at[4]),
    ]
    load_out = [
        pltpu.make_async_copy(wo, wout.at[pl.ds(0, q_rows), :], w_sem.at[5]),
        pltpu.make_async_copy(wpo, wout.at[pl.ds(q_rows, 4 * channels), :], w_sem.at[6]),
    ]
    load_sink = pltpu.make_async_copy(sink_hbm, sink, w_sem.at[7])
    for c in reversed(range(chunks)):
        local_tokens(c).start()
    load_gain.start()
    load_wp.start(priority=1)
    for load in loads + load_out:
        load.start(priority=1)
    load_sink.start()

    with scope("barrier"):

        @pl.when(me_tp == 0)
        def _():
            pl.semaphore_wait(barrier, 1)
            pl.semaphore_signal(ready.at[0], inc=1, device_id={"tp": 1}, device_id_type=MESH)

        @pl.when(me_tp == 1)
        def _():
            pl.semaphore_wait(ready.at[0], 1)

    remote_tokens(chunks - 1).start()
    for step in range(1, n_sp):

        @pl.when((me_tp == 1) & (me_sp - step >= 0))
        def _():
            pl.semaphore_signal(
                barrier,
                inc=1,
                device_id={"sp": lax.rem(me_sp - step + n_sp, n_sp)},
                device_id_type=MESH,
            )

    target = lax.broadcasted_iota(jnp.int32, (WINDOW, 2 * WINDOW), 0) + WINDOW
    source = lax.broadcasted_iota(jnp.int32, (WINDOW, 2 * WINDOW), 1)
    gap = target - source
    for g, reach in enumerate(REACHES):
        bands[g] = jnp.where((gap >= 0) & (gap < reach), 1.0, 0.0).astype(BF16)
    bands[3] = jnp.where((gap >= 0) & (gap < WINDOW) & (source >= WINDOW), 1.0, 0.0).astype(BF16)
    own_key = lax.broadcasted_iota(jnp.int32, (WINDOW, PAIR * WINDOW), 0) <= lax.rem(
        lax.broadcasted_iota(jnp.int32, (WINDOW, PAIR * WINDOW), 1), jnp.int32(WINDOW)
    )
    tri[...] = jnp.where(own_key, 1.0, 0.0).astype(BF16)
    ext[pl.ds(0, WINDOW - TAIL), :] = jnp.zeros((WINDOW - TAIL, pool_cols), BF16)

    @pl.when(me_sp == 0)
    def _():
        ext[pl.ds(WINDOW - TAIL, TAIL), :] = jnp.zeros((TAIL, pool_cols), BF16)
        keys[0] = jnp.zeros((WINDOW, kv_rows), BF16)
        vals[0] = jnp.zeros((kv_rows, WINDOW), BF16)

    def halo_copy(src, dst, index):
        return pltpu.make_async_remote_copy(
            src_ref=src,
            dst_ref=dst,
            send_sem=halo_send.at[index],
            recv_sem=halo_recv.at[index],
            device_id={"sp": lax.rem(me_sp + 1, n_sp)},
            device_id_type=MESH,
        )

    halos = [
        halo_copy(keys.at[blocks], keys.at[0], 0),
        halo_copy(vals.at[blocks], vals.at[0], 1),
        halo_copy(
            ext.at[pl.ds(WINDOW + rows - TAIL, TAIL), :],
            ext.at[pl.ds(WINDOW - TAIL, TAIL), :],
            2,
        ),
    ]

    def total_copy(step):
        return pltpu.make_async_remote_copy(
            src_ref=totals.at[me_sp],
            dst_ref=totals.at[me_sp],
            send_sem=tot_send.at[step],
            recv_sem=tot_recv.at[step],
            device_id={"sp": lax.rem(me_sp + step, n_sp)},
            device_id_type=MESH,
        )

    scale = head_dim ** (-0.5)

    def qkv(c, source):
        half = wqkv.shape[0] // 2
        low = dot(wqkv[pl.ds(0, half), :], source, ((1,), (1,)))
        high = dot(wqkv[pl.ds(half, half), :], source, ((1,), (1,)))
        split = q_rows - half
        for j in range(per_chunk):
            b = c * per_chunk + j
            at = slice(j * WINDOW, (j + 1) * WINDOW)
            qt[b, pl.ds(0, half), :] = (low[:, at] * scale).astype(BF16)
            qt[b, pl.ds(half, split), :] = (high[:split, at] * scale).astype(BF16)
            keys[b + 1] = high[split : split + kv_rows, at].T.astype(BF16)
            vals[b + 1] = high[split + kv_rows :, at].astype(BF16)

    def ext_chunk(c):
        return ext.at[pl.ds(WINDOW + c * CHUNK, CHUNK), :]

    none = jnp.zeros((head_dim, PAIR * WINDOW), BF16)

    def unit_scores(unit):
        b, h, p, edge = unit
        first_head = h * group + p * PAIR
        q = jnp.concatenate(
            [qt[b, pl.ds((first_head + g) * head_dim, head_dim), :] for g in range(PAIR)],
            axis=1,
        )
        rhs = jnp.concatenate([q if k == h else none for k in range(local_kv)], axis=0)
        return dot(keys[b], rhs), dot(keys[b + 1], rhs)

    def unit_weights(unit, scores):
        b, h, p, edge = unit
        first_head = h * group + p * PAIR
        before, own = scores
        if edge:
            before = before + jnp.where((b == 0) & (me_sp == 0), -jnp.inf, 0.0).astype(F32)
        s = jnp.concatenate(
            [jnp.full((1, WINDOW), sink[first_head + g], F32) for g in range(PAIR)], axis=1
        )
        score = jnp.where(own_key, own, before)
        top = jnp.maximum(jnp.max(score, axis=0, keepdims=True), s)
        expo = jnp.exp(score - top)
        total = jnp.sum(expo, axis=0, keepdims=True) + jnp.exp(s - top)
        weight = (expo * (1.0 / total)).astype(BF16)
        w_own = weight * tri[...]
        return jnp.concatenate([weight - w_own, w_own], axis=0)

    def block_rows(b):
        return pl.ds(pl.multiple_of(b * WINDOW, WINDOW), WINDOW)

    def unit_output(unit, weights):
        b, h, p, edge = unit
        first_head = h * group + p * PAIR
        v_at = pl.ds(h * head_dim, head_dim)
        v = jnp.concatenate([vals[b, v_at, :], vals[b + 1, v_at, :]], axis=1)
        gathered = dot(v, weights)
        stacked = jnp.concatenate(
            [gathered[:, g * WINDOW : (g + 1) * WINDOW] for g in range(PAIR)], axis=0
        )
        act[block_rows(b), pl.ds(first_head * head_dim, PAIR * head_dim)] = stacked.T.astype(BF16)

    ascending = [blocks - 1, 1, 2, 0] + list(range(3, blocks - 1))
    sequence = [either(blocks - 1 - i, ascending[i]) for i in range(blocks)]
    units = [
        (sequence[i], h, p, 0 in (blocks - 1 - i, ascending[i]))
        for i in range(blocks)
        for h in range(local_kv)
        for p in range(group // PAIR)
    ]
    per_block = len(units) // blocks
    scores, weights = {}, {}

    def score(first, count):
        for u in range(first, first + count):
            scores[u] = unit_scores(units[u])

    def soften(first, count):
        for u in range(first, first + count):
            weights[u] = unit_weights(units[u], scores.pop(u))

    def gather(first, count):
        for u in range(first, first + count):
            unit_output(units[u], weights.pop(u))

    def pool(b, groups, carried=None):
        start = pl.multiple_of(b * WINDOW, WINDOW)
        position = me_sp * rows + b * WINDOW + 1
        count = (lax.broadcasted_iota(jnp.int32, (WINDOW, channels), 0) + position).astype(F32)
        for g in groups:
            col = pl.ds(g * channels, channels)
            own = ext[pl.ds(start + WINDOW, WINDOW), col]
            if g < 3:
                sums = dot(bands[g], ext[pl.ds(start, 2 * WINDOW), col])
                denom = jnp.minimum(count, float(REACHES[g]))
            else:
                base = carried
                for earlier in range(blocks):
                    base = base + jnp.where(earlier < b, block_sum[earlier], 0.0)
                sums = dot(bands[3, :, pl.ds(WINDOW, WINDOW)], own) + base[:1]
                denom = count
            pooled = sums * (1.0 / denom) - own.astype(F32)
            act[block_rows(b), pl.ds(q_rows + g * channels, channels)] = pooled.astype(BF16)

    def columns(t):
        return pl.ds(t * COLS, COLS)

    def partial_send(t):
        left = t < left_tiles
        return pltpu.make_async_remote_copy(
            src_ref=sending.at[t],
            dst_ref=landing_left.at[t] if left else landing_right.at[t - left_tiles],
            send_sem=out_send.at[t],
            recv_sem=out_recv.at[t],
            device_id={"tp": other},
            device_id_type=MESH,
        )

    with scope("send_tokens"):
        for c in reversed(range(chunks - 1)):
            local_tokens(c).wait()
            remote_tokens(c).start()
    with scope("wait_wp"):
        load_wp.wait()
    part = wp_f32.shape[0]

    def regroup(i, carry):
        wp_f32[...] = wp_raw[pl.ds(pl.multiple_of(i * part, part), part), :].astype(F32)
        at = pl.ds(pl.multiple_of(i * (part // 4), part // 4), part // 4)
        for g in range(4):
            wpool[at, pl.ds(g * channels, channels)] = wp_f32[
                pl.ds(g, part // 4, stride=4), :
            ].astype(BF16)
        return carry

    def normalize_chunk(c):
        normalize(tok.at[c, 0], tok.at[c, 1], gain, store_into(normed.at[c]))

    with scope("regroup"):
        lax.fori_loop(0, wp_raw.shape[0] // part, regroup, 0)
    with scope("wait_tokens"):
        load_gain.wait()
        local_tokens(chunks - 1).wait()
        remote_tokens(chunks - 1).wait_recv()
    with scope("normalize"):
        normalize_chunk(chunks - 1)
    for c in reversed(range(chunks)):
        if c > 0:
            with scope("wait_tokens"):
                remote_tokens(c - 1).wait_recv()
        with scope("pool_proj"):
            project_pool(
                normed.at[c], wpool, ext_chunk(c), block_sum.at[pl.ds(c * per_chunk, per_chunk)]
            )
            if c > 0:
                normalize_chunk(c - 1)
    all_rows = block_sum[0]
    for b in range(1, blocks):
        all_rows = all_rows + block_sum[b]
    totals[me_sp] = all_rows
    with scope("sp_ready"):

        @pl.when(me_sp < n_sp - 1)
        def _():
            @pl.when(me_tp == 1)
            def _():
                pl.semaphore_wait(barrier, n_sp - 1 - me_sp)
                pl.semaphore_signal(ready.at[1], inc=1, device_id={"tp": 0}, device_id_type=MESH)

            @pl.when(me_tp == 0)
            def _():
                pl.semaphore_wait(ready.at[1], 1)

    for step in range(1, n_sp):

        @pl.when(me_sp + step < n_sp)
        def _():
            total_copy(step).start()

    with scope("wait_wqkv"):
        for load in loads:
            load.wait()
    with scope("qkv_first"):
        qkv(chunks - 1, normed[chunks - 1])

    @pl.when(me_sp < n_sp - 1)
    def _():
        for halo in halos:
            halo.start()

    load_sink.wait()
    give_first = other * half_blocks
    keep_first = me_tp * half_blocks

    def half_of(first):
        return act[pl.ds(pl.multiple_of(first * WINDOW, WINDOW), half_rows), :]

    quarter = COLS // 2

    def give(t, part):
        at = pl.ds(t * COLS + part * quarter, quarter)
        sending[t, :, pl.ds(part * quarter, quarter)] = dot(
            half_of(give_first), wout[:, at]
        ).astype(BF16)

    for i in range(1, chunks):
        c = either(chunks - 1 - i, i - 1)
        with scope("qkv_rest"):
            first = (i - 1) * per_block
            score(first, per_block)
            qkv(c, normed[c])
            soften(first, per_block)
            gather(first, per_block)
    with scope("attend_a"):
        first = (chunks - 1) * per_block
        score(first, per_block)
        pairs = [(i, g) for i in range(half_blocks) for g in range(3)]

    def wait_halo(tp):
        with scope("wait_halo"):

            @pl.when((me_sp > 0) & (me_tp == tp))
            def _():
                for halo in halos:
                    halo.wait_recv()

    wait_halo(1)
    with scope("attend_b"):
        soften(first, per_block)
        score(first + per_block, per_block)
        gather(first, per_block)
        for i, g in pairs:
            pool(give_first + i, (g,))
        soften(first + per_block, per_block)
        gather(first + per_block, per_block)
    with scope("wait_totals"):
        for step in range(1, n_sp):

            @pl.when(me_sp - step >= 0)
            def _():
                total_copy(step).wait_recv()

    carried = jnp.zeros((8, channels), F32)
    for index in range(n_sp):
        carried = carried + jnp.where(index < me_sp, totals[index], 0.0)
    first = first + 2 * per_block
    left = len(units) - first
    with scope("pool_b"):
        score(first, left // tiles)
        for i in range(half_blocks):
            pool(give_first + i, (3,), carried)

    keep_pieces = [(i, g) for i in reversed(range(half_blocks)) for g in range(4)]
    for load in load_out:
        load.wait()
    for t in range(tiles):
        if t == 1:
            wait_halo(0)
        with scope("give"):
            lo, hi = first + t * left // tiles, first + (t + 1) * left // tiles
            for part in range(2):
                give(t, part)
            soften(lo, hi - lo)
            if t < tiles - 1:
                score(hi, first + (t + 2) * left // tiles - hi)
            gather(lo, hi - lo)
            at = [len(keep_pieces) * k // tiles for k in (t, t + 1)]
            for i, g in keep_pieces[at[0] : at[1]]:
                pool(keep_first + i, (g,), carried)
        partial_send(t).start()
    with scope("wait_give"):
        for t in range(left_tiles):
            partial_send(t).wait_recv()
    with scope("keep"):
        for t in range(left_tiles):
            mine = dot(half_of(keep_first), wout[:, columns(t)])
            out_left[:, columns(t)] = (mine + landing_left[t].astype(F32)).astype(BF16)
    with scope("end_mix"):
        for t in range(left_tiles, tiles):
            partial_send(t).wait_recv()
        for t in range(tiles):
            partial_send(t).wait_send()
        for c in range(chunks):
            remote_tokens(c).wait_send()
        for step in range(1, n_sp):

            @pl.when(me_sp + step < n_sp)
            def _():
                total_copy(step).wait_send()

        @pl.when(me_sp < n_sp - 1)
        def _():
            for halo in halos:
                halo.wait_send()


def finish_kernel(act, wout, out_left, landing_right, out, out_right, sem):
    me_tp = lax.axis_index("tp")
    half_rows, left_width = out_left.shape
    right_tiles = landing_right.shape[0]
    left = pltpu.make_async_copy(out_left, out.at[:, pl.ds(0, left_width)], sem.at[0])
    left.start()

    def right(t):
        at = pl.ds(left_width + t * COLS, COLS)
        return pltpu.make_async_copy(out_right.at[t], out.at[:, at], sem.at[1 + t])

    mine = act[pl.ds(pl.multiple_of(me_tp * half_rows, half_rows), half_rows), :]
    for t in range(right_tiles):
        at = pl.ds(left_width + t * COLS, COLS)
        out_right[t] = (dot(mine, wout[:, at]) + landing_right[t].astype(F32)).astype(BF16)
        right(t).start()
    left.wait()
    for t in range(right_tiles):
        right(t).wait()


def shards(n_sp, tokens, gain, wq, wk, wv, sink, wp, wo, wpo):
    rows, half_width = tokens.shape[1:]
    width = 2 * half_width
    heads, head_dim = wq.shape[1:]
    local_kv = wk.shape[1]
    channels = wp.shape[2]
    q_rows, kv_rows = (heads * head_dim, local_kv * head_dim)
    pool_cols = 4 * channels
    blocks = rows // WINDOW
    tiles = width // COLS
    left_tiles = tiles - 1
    chunks = rows // CHUNK
    per_chunk = CHUNK // WINDOW
    half_rows = rows // 2
    dma = pltpu.SemaphoreType.DMA
    flat = lambda w: jnp.transpose(w, (1, 2, 0)).reshape(-1, width)
    hbm = pl.BlockSpec(memory_space=pltpu.HBM)
    vmem = pl.BlockSpec(memory_space=pltpu.VMEM)

    mixed = [
        ((rows, q_rows + pool_cols), BF16),
        ((half_rows, left_tiles * COLS), BF16),
        ((tiles - left_tiles, half_rows, COLS), BF16),
        ((q_rows + pool_cols, width), BF16),
    ]
    size = lambda shapes: sum(
        functools.reduce(lambda a, b: a * b, s) * jnp.dtype(d).itemsize for s, d in shapes
    )
    spare = 67043328 - 262144
    act, out_left, landing_right, wout = pl.pallas_call(
        functools.partial(mix_kernel, n_sp, heads, local_kv, head_dim),
        out_shape=[pltpu.VMEM(s, d) for s, d in mixed],
        in_specs=[hbm] * 9,
        out_specs=[vmem] * len(mixed),
        scratch_shapes=[
            pltpu.VMEM((chunks, 2, CHUNK, half_width), BF16),
            pltpu.VMEM((chunks, CHUNK, width), BF16),
            pltpu.VMEM((1, width), F32),
            pltpu.SMEM((heads,), F32),
            pltpu.VMEM((4 * width, channels), BF16),
            pltpu.VMEM((1024, channels), F32),
            pltpu.VMEM((width, pool_cols), BF16),
            pltpu.VMEM((q_rows + 2 * kv_rows, width), BF16),
            pltpu.VMEM((WINDOW, PAIR * WINDOW), BF16),
            pltpu.VMEM((4, WINDOW, 2 * WINDOW), BF16),
            pltpu.VMEM((blocks, q_rows, WINDOW), BF16),
            pltpu.VMEM((blocks + 1, WINDOW, kv_rows), BF16),
            pltpu.VMEM((blocks + 1, kv_rows, WINDOW), BF16),
            pltpu.VMEM((rows + WINDOW, pool_cols), BF16),
            pltpu.VMEM((blocks, 8, channels), F32),
            pltpu.VMEM((n_sp, 8, channels), F32),
            pltpu.VMEM((tiles, half_rows, COLS), BF16),
            pltpu.VMEM((left_tiles, half_rows, COLS), BF16),
            dma((8,)),
            dma((chunks,)),
            dma((chunks,)),
            dma((chunks,)),
            dma((3,)),
            dma((3,)),
            dma((n_sp,)),
            dma((n_sp,)),
            dma((tiles,)),
            dma((tiles,)),
            pltpu.SemaphoreType.REGULAR((2,)),
        ],
        compiler_params=pltpu.CompilerParams(
            collective_id=0, has_side_effects=True, vmem_limit_bytes=spare - size(mixed)
        ),
    )(
        tokens[0],
        gain.reshape(1, width),
        flat(wq),
        flat(wk),
        flat(wv),
        wp.reshape(-1, channels),
        wo.reshape(-1, width),
        wpo.reshape(-1, width),
        sink,
    )
    result = pl.pallas_call(
        finish_kernel,
        out_shape=jax.ShapeDtypeStruct((half_rows, width), BF16),
        in_specs=[vmem] * 4,
        out_specs=hbm,
        scratch_shapes=[
            pltpu.VMEM((tiles - left_tiles, half_rows, COLS), BF16),
            dma((1 + tiles - left_tiles,)),
        ],
        compiler_params=pltpu.CompilerParams(vmem_limit_bytes=spare // 3),
    )(act, wout, out_left, landing_right)
    return result[None]


def solution(mesh):
    in_specs = (
        P("fs", ("grp", "sp"), "tp"),
        P(),
        P(None, "tp", None),
        P(None, "tp", None),
        P(None, "tp", None),
        P("tp"),
        P(None, None, "tp"),
        P("tp", None, None),
        P(None, "tp", None),
    )
    out_specs = P("fs", ("grp", "sp", "tp"), None)
    return jax.shard_map(
        functools.partial(shards, mesh.shape["sp"]),
        mesh=mesh,
        in_specs=in_specs,
        out_specs=out_specs,
        check_vma=False,
    )
```

time: 20.1 us -> 18.2 us (0.905)
  the two profiles are of different devices: /device:TPU:0 before, /device:TPU:11 now
where the time goes in v2:
time: 18.2 us; the launch traced here: 18 us
  Pallas kernels  18 us (99%)
    pallas_call x1, Pallas kernels, shards(): pl.pallas_call(functools.partial(mix_kernel, n_sp, heads, local_kv, head_...  16.7 us
    pallas_call x1, Pallas kernels, shards(): pl.pallas_call(finish_kernel, out_shape=jax.ShapeDtypeStruct((half_rows,...  1.34 us

profile of v2, /device:TPU:11, one launch (start us, length us, event | category | flops | bytes accessed | tf_op | source)
XLA Modules:
  0.0 18.0 jit_solution(13859760821499270666)
XLA Ops:
  0.0 16.7 %shard_map.91 = (bf16[768,1024]{1,0:T(8,128)(2,1)S(1)}, bf16[384,1536]{1,0:T(8,128)(2,1)S(1)}, bf16[1,384,512]{2,1,0:T(8,128)(2,1)S(1)}, bf16[1024,2048]{1,0:T(8,128)(2,1)S(1)}) custom-call(bf16[768,1024]{1,0:T(8,128)(2,1)} %bitcast.19, f32[1,2048]{1,0:T(1,128)} %bitcast.22, bf16[512,2048]{1,0:T(8,128)(2,1)} %bitcast.15, bf16[128,2048]{1,0:T(8,128)(2,1)} %bitcast.20, ...), custom_call_target="tpu_custom_call" | custom-call | tf_op jit(solution)/shard_map/pallas_call | solution.py:584
  16.7 1.3 %shard_map.92 = bf16[384,2048]{1,0:T(8,128)(2,1)} custom-call(bf16[768,1024]{1,0:T(8,128)(2,1)S(1)} %get-tuple-element.9.act, bf16[1024,2048]{1,0:T(8,128)(2,1)S(1)} %get-tuple-element.10.wout, bf16[384,1536]{1,0:T(8,128)(2,1)S(1)} %get-tuple-element.11.out_left, bf16[1,384,512]{2,1,0:T(8,128)(2,1)S(1)} %get-tuple-element.12.landing_right), custom_call_target="tpu_custom_call" | custom-call | tf_op jit(solution)/shard_map/pallas_call | solution.py:634

commit v3 on v2

--- a/solution.py
+++ b/solution.py
@@ -160,8 +160,7 @@
     for c in reversed(range(chunks)):
         local_tokens(c).start()
     load_gain.start()
-    load_wp.start(priority=1)
-    for load in loads + load_out:
+    for load in loads + [load_wp] + load_out:
         load.start(priority=1)
     load_sink.start()
 
@@ -297,7 +296,7 @@
         )
         act[block_rows(b), pl.ds(first_head * head_dim, PAIR * head_dim)] = stacked.T.astype(BF16)
 
-    ascending = [blocks - 1, 1, 2, 0] + list(range(3, blocks - 1))
+    ascending = [blocks - 1, 1, 0] + list(range(2, blocks - 1))
     sequence = [either(blocks - 1 - i, ascending[i]) for i in range(blocks)]
     units = [
         (sequence[i], h, p, 0 in (blocks - 1 - i, ascending[i]))
@@ -357,44 +356,42 @@
         for c in reversed(range(chunks - 1)):
             local_tokens(c).wait()
             remote_tokens(c).start()
-    with scope("wait_wp"):
-        load_wp.wait()
-    part = wp_f32.shape[0]
-
-    def regroup(i, carry):
-        wp_f32[...] = wp_raw[pl.ds(pl.multiple_of(i * part, part), part), :].astype(F32)
-        at = pl.ds(pl.multiple_of(i * (part // 4), part // 4), part // 4)
+    part = 4 * CHUNK
+
+    def regroup(i):
+        rows_at = pl.ds(i * part, part)
+        wp_f32[rows_at, :] = wp_raw[rows_at, :].astype(F32)
         for g in range(4):
-            wpool[at, pl.ds(g * channels, channels)] = wp_f32[
-                pl.ds(g, part // 4, stride=4), :
+            wpool[pl.ds(i * CHUNK, CHUNK), pl.ds(g * channels, channels)] = wp_f32[
+                pl.ds(i * part + g, CHUNK, stride=4), :
             ].astype(BF16)
-        return carry
 
     def normalize_chunk(c):
         normalize(tok.at[c, 0], tok.at[c, 1], gain, store_into(normed.at[c]))
 
-    with scope("regroup"):
-        lax.fori_loop(0, wp_raw.shape[0] // part, regroup, 0)
     with scope("wait_tokens"):
         load_gain.wait()
         local_tokens(chunks - 1).wait()
         remote_tokens(chunks - 1).wait_recv()
     with scope("normalize"):
         normalize_chunk(chunks - 1)
-    for c in reversed(range(chunks)):
-        if c > 0:
-            with scope("wait_tokens"):
-                remote_tokens(c - 1).wait_recv()
-        with scope("pool_proj"):
-            project_pool(
-                normed.at[c], wpool, ext_chunk(c), block_sum.at[pl.ds(c * per_chunk, per_chunk)]
-            )
-            if c > 0:
-                normalize_chunk(c - 1)
-    all_rows = block_sum[0]
-    for b in range(1, blocks):
-        all_rows = all_rows + block_sum[b]
-    totals[me_sp] = all_rows
+    def pool_chunk(c):
+        project_pool(
+            normed.at[c], wpool, ext_chunk(c), block_sum.at[pl.ds(c * per_chunk, per_chunk)]
+        )
+
+    with scope("wait_wqkv"):
+        for load in loads:
+            load.wait()
+    with scope("wait_wp"):
+        load_wp.wait()
+        remote_tokens(chunks - 2).wait_recv()
+    with scope("first"):
+        qkv(chunks - 1, normed[chunks - 1])
+        for i in range(wp_raw.shape[0] // part):
+            regroup(i)
+        normalize_chunk(chunks - 2)
+        pool_chunk(chunks - 1)
     with scope("sp_ready"):
 
         @pl.when(me_sp < n_sp - 1)
@@ -408,23 +405,30 @@
             def _():
                 pl.semaphore_wait(ready.at[1], 1)
 
-    for step in range(1, n_sp):
-
-        @pl.when(me_sp + step < n_sp)
-        def _():
-            total_copy(step).start()
-
-    with scope("wait_wqkv"):
-        for load in loads:
-            load.wait()
-    with scope("qkv_first"):
-        qkv(chunks - 1, normed[chunks - 1])
-
     @pl.when(me_sp < n_sp - 1)
     def _():
         for halo in halos:
             halo.start()
 
+    with scope("wait_tokens"):
+        for c in reversed(range(chunks - 2)):
+            remote_tokens(c).wait_recv()
+    with scope("pool_proj"):
+        for c in reversed(range(chunks - 1)):
+            pool_chunk(c)
+            if c > 0:
+                normalize_chunk(c - 1)
+        all_rows = block_sum[0]
+        for b in range(1, blocks):
+            all_rows = all_rows + block_sum[b]
+        totals[me_sp] = all_rows
+
+    for step in range(1, n_sp):
+
+        @pl.when(me_sp + step < n_sp)
+        def _():
+            total_copy(step).start()
+
     load_sink.wait()
     give_first = other * half_blocks
     keep_first = me_tp * half_blocks
@@ -432,26 +436,8 @@
     def half_of(first):
         return act[pl.ds(pl.multiple_of(first * WINDOW, WINDOW), half_rows), :]
 
-    quarter = COLS // 2
-
-    def give(t, part):
-        at = pl.ds(t * COLS + part * quarter, quarter)
-        sending[t, :, pl.ds(part * quarter, quarter)] = dot(
-            half_of(give_first), wout[:, at]
-        ).astype(BF16)
-
-    for i in range(1, chunks):
-        c = either(chunks - 1 - i, i - 1)
-        with scope("qkv_rest"):
-            first = (i - 1) * per_block
-            score(first, per_block)
-            qkv(c, normed[c])
-            soften(first, per_block)
-            gather(first, per_block)
-    with scope("attend_a"):
-        first = (chunks - 1) * per_block
-        score(first, per_block)
-        pairs = [(i, g) for i in range(half_blocks) for g in range(3)]
+    def give(t):
+        sending[t] = dot(half_of(give_first), wout[:, columns(t)]).astype(BF16)
 
     def wait_halo(tp):
         with scope("wait_halo"):
@@ -461,15 +447,27 @@
                 for halo in halos:
                     halo.wait_recv()
 
-    wait_halo(1)
-    with scope("attend_b"):
+    first = 0
+    for i in range(1, chunks):
+        c = either(chunks - 1 - i, i - 1)
+        count = per_block * i
+        if i == chunks - 1:
+            wait_halo(1)
+        with scope("qkv_rest"):
+            score(first, count)
+            soften(first, count)
+            qkv(c, normed[c])
+            gather(first, count)
+        first += count
+
+    with scope("attend_a"):
+        score(first, per_block)
         soften(first, per_block)
-        score(first + per_block, per_block)
+        for i in range(half_blocks):
+            for g in range(3):
+                pool(give_first + i, (g,))
         gather(first, per_block)
-        for i, g in pairs:
-            pool(give_first + i, (g,))
-        soften(first + per_block, per_block)
-        gather(first + per_block, per_block)
+    first += per_block
     with scope("wait_totals"):
         for step in range(1, n_sp):
 
@@ -480,7 +478,6 @@
     carried = jnp.zeros((8, channels), F32)
     for index in range(n_sp):
         carried = carried + jnp.where(index < me_sp, totals[index], 0.0)
-    first = first + 2 * per_block
     left = len(units) - first
     with scope("pool_b"):
         score(first, left // tiles)
@@ -495,12 +492,11 @@
             wait_halo(0)
         with scope("give"):
             lo, hi = first + t * left // tiles, first + (t + 1) * left // tiles
-            for part in range(2):
-                give(t, part)
             soften(lo, hi - lo)
+            give(t)
+            gather(lo, hi - lo)
             if t < tiles - 1:
                 score(hi, first + (t + 2) * left // tiles - hi)
-            gather(lo, hi - lo)
             at = [len(keep_pieces) * k // tiles for k in (t, t + 1)]
             for i, g in keep_pieces[at[0] : at[1]]:
                 pool(keep_first + i, (g,), carried)
@@ -592,7 +588,7 @@
             pltpu.VMEM((1, width), F32),
             pltpu.SMEM((heads,), F32),
             pltpu.VMEM((4 * width, channels), BF16),
-            pltpu.VMEM((1024, channels), F32),
+            pltpu.VMEM((4 * width, channels), F32),
             pltpu.VMEM((width, pool_cols), BF16),
             pltpu.VMEM((q_rows + 2 * kv_rows, width), BF16),
             pltpu.VMEM((WINDOW, PAIR * WINDOW), BF16),

time: 18.2 us -> 17.9 us (0.984)
  the two profiles are of different devices: /device:TPU:11 before, /device:TPU:9 now
where the time goes in v3:
time: 17.9 us; the launch traced here: 17.7 us
  Pallas kernels  17.7 us (99%)
    pallas_call x1, Pallas kernels, shards(): pl.pallas_call(functools.partial(mix_kernel, n_sp, heads, local_kv, head_...  16.4 us
    pallas_call x1, Pallas kernels, shards(): pl.pallas_call(finish_kernel, out_shape=jax.ShapeDtypeStruct((half_rows,...  1.34 us

profile of v3, /device:TPU:9, one launch (start us, length us, event | category | flops | bytes accessed | tf_op | source)
XLA Modules:
  0.0 17.7 jit_solution(4976494876075834708)
XLA Ops:
  0.0 16.4 %shard_map.91 = (bf16[768,1024]{1,0:T(8,128)(2,1)S(1)}, bf16[384,1536]{1,0:T(8,128)(2,1)S(1)}, bf16[1,384,512]{2,1,0:T(8,128)(2,1)S(1)}, bf16[1024,2048]{1,0:T(8,128)(2,1)S(1)}) custom-call(bf16[768,1024]{1,0:T(8,128)(2,1)} %bitcast.19, f32[1,2048]{1,0:T(1,128)} %bitcast.22, bf16[512,2048]{1,0:T(8,128)(2,1)} %bitcast.15, bf16[128,2048]{1,0:T(8,128)(2,1)} %bitcast.20, ...), custom_call_target="tpu_custom_call" | custom-call | tf_op jit(solution)/shard_map/pallas_call | solution.py:580
  16.4 1.3 %shard_map.92 = bf16[384,2048]{1,0:T(8,128)(2,1)} custom-call(bf16[768,1024]{1,0:T(8,128)(2,1)S(1)} %get-tuple-element.9.act, bf16[1024,2048]{1,0:T(8,128)(2,1)S(1)} %get-tuple-element.10.wout, bf16[384,1536]{1,0:T(8,128)(2,1)S(1)} %get-tuple-element.11.out_left, bf16[1,384,512]{2,1,0:T(8,128)(2,1)S(1)} %get-tuple-element.12.landing_right), custom_call_target="tpu_custom_call" | custom-call | tf_op jit(solution)/shard_map/pallas_call | solution.py:630

commit v4 on v3

--- a/solution.py
+++ b/solution.py
@@ -14,6 +14,7 @@
 CHUNK = 256
 COLS = 512
 PAIR = 2
+LEAD_PARTS = 2
 F32 = jnp.float32
 BF16 = jnp.bfloat16
 scope = jax.named_scope
@@ -134,15 +135,27 @@
             tokens.at[pl.ds(c * CHUNK, CHUNK), :], tok.at[c, me_tp], tok_sem.at[c]
         )
 
-    def remote_tokens(c):
-        direct = c == chunks - 1
+    def token_copy(source, where, index):
         return pltpu.make_async_remote_copy(
-            src_ref=tokens.at[pl.ds(c * CHUNK, CHUNK), :] if direct else tok.at[c, me_tp],
-            dst_ref=tok.at[c, me_tp],
-            send_sem=tok_send.at[c],
-            recv_sem=tok_recv.at[c],
+            src_ref=source,
+            dst_ref=where,
+            send_sem=tok_send.at[index],
+            recv_sem=tok_recv.at[index],
             device_id={"tp": other},
             device_id_type=MESH,
+        )
+
+    def remote_tokens(c):
+        return token_copy(tok.at[c, me_tp], tok.at[c, me_tp], c)
+
+    lead = chunks - 1
+    piece = CHUNK // LEAD_PARTS
+
+    def remote_lead(k):
+        return token_copy(
+            tokens.at[pl.ds(lead * CHUNK + k * piece, piece), :],
+            tok.at[lead, me_tp, pl.ds(k * piece, piece), :],
+            lead + k,
         )
 
     load_wp = pltpu.make_async_copy(wp, wp_raw, w_sem.at[0])
@@ -175,7 +188,8 @@
         def _():
             pl.semaphore_wait(ready.at[0], 1)
 
-    remote_tokens(chunks - 1).start()
+    for k in range(LEAD_PARTS):
+        remote_lead(k).start()
     for step in range(1, n_sp):
 
         @pl.when((me_tp == 1) & (me_sp - step >= 0))
@@ -371,10 +385,18 @@
 
     with scope("wait_tokens"):
         load_gain.wait()
-        local_tokens(chunks - 1).wait()
-        remote_tokens(chunks - 1).wait_recv()
-    with scope("normalize"):
-        normalize_chunk(chunks - 1)
+        local_tokens(lead).wait()
+    for k in range(LEAD_PARTS):
+        with scope("wait_tokens"):
+            remote_lead(k).wait_recv()
+        with scope("normalize"):
+            at = pl.ds(k * piece, piece)
+            normalize(
+                tok.at[lead, 0, at, :],
+                tok.at[lead, 1, at, :],
+                gain,
+                store_into(normed.at[lead, at, :]),
+            )
     def pool_chunk(c):
         project_pool(
             normed.at[c], wpool, ext_chunk(c), block_sum.at[pl.ds(c * per_chunk, per_chunk)]
@@ -383,11 +405,12 @@
     with scope("wait_wqkv"):
         for load in loads:
             load.wait()
+    with scope("lead_qkv"):
+        qkv(lead, normed[lead])
     with scope("wait_wp"):
         load_wp.wait()
         remote_tokens(chunks - 2).wait_recv()
     with scope("first"):
-        qkv(chunks - 1, normed[chunks - 1])
         for i in range(wp_raw.shape[0] // part):
             regroup(i)
         normalize_chunk(chunks - 2)
@@ -501,20 +524,23 @@
             for i, g in keep_pieces[at[0] : at[1]]:
                 pool(keep_first + i, (g,), carried)
         partial_send(t).start()
-    with scope("wait_give"):
-        for t in range(left_tiles):
-            partial_send(t).wait_recv()
-    with scope("keep"):
-        for t in range(left_tiles):
-            mine = dot(half_of(keep_first), wout[:, columns(t)])
-            out_left[:, columns(t)] = (mine + landing_left[t].astype(F32)).astype(BF16)
+    for group_tiles in (range(left_tiles - 1), range(left_tiles - 1, left_tiles)):
+        with scope("wait_give"):
+            for t in group_tiles:
+                partial_send(t).wait_recv()
+        with scope("keep"):
+            for t in group_tiles:
+                mine = dot(half_of(keep_first), wout[:, columns(t)])
+                out_left[:, columns(t)] = (mine + landing_left[t].astype(F32)).astype(BF16)
     with scope("end_mix"):
         for t in range(left_tiles, tiles):
             partial_send(t).wait_recv()
         for t in range(tiles):
             partial_send(t).wait_send()
-        for c in range(chunks):
+        for c in range(lead):
             remote_tokens(c).wait_send()
+        for k in range(LEAD_PARTS):
+            remote_lead(k).wait_send()
         for step in range(1, n_sp):
 
             @pl.when(me_sp + step < n_sp)
@@ -603,8 +629,8 @@
             pltpu.VMEM((left_tiles, half_rows, COLS), BF16),
             dma((8,)),
             dma((chunks,)),
-            dma((chunks,)),
-            dma((chunks,)),
+            dma((chunks - 1 + LEAD_PARTS,)),
+            dma((chunks - 1 + LEAD_PARTS,)),
             dma((3,)),
             dma((3,)),
             dma((n_sp,)),

time: 17.9 us -> 16.9 us (0.944)
  the two profiles are of different devices: /device:TPU:9 before, /device:TPU:0 now
where the time goes in v4:
time: 16.9 us; the launch traced here: 16.7 us
  Pallas kernels  16.7 us (99%)
    pallas_call x1, Pallas kernels, shards(): pl.pallas_call(functools.partial(mix_kernel, n_sp, heads, local_kv, head_...  15.4 us
    pallas_call x1, Pallas kernels, shards(): pl.pallas_call(finish_kernel, out_shape=jax.ShapeDtypeStruct((half_rows,...  1.34 us

profile of v4, /device:TPU:0, one launch (start us, length us, event | category | flops | bytes accessed | tf_op | source)
XLA Modules:
  0.0 16.7 jit_solution(12377718629570338710)
XLA Ops:
  0.0 15.4 %shard_map.91 = (bf16[768,1024]{1,0:T(8,128)(2,1)S(1)}, bf16[384,1536]{1,0:T(8,128)(2,1)S(1)}, bf16[1,384,512]{2,1,0:T(8,128)(2,1)S(1)}, bf16[1024,2048]{1,0:T(8,128)(2,1)S(1)}) custom-call(bf16[768,1024]{1,0:T(8,128)(2,1)} %bitcast.19, f32[1,2048]{1,0:T(1,128)} %bitcast.22, bf16[512,2048]{1,0:T(8,128)(2,1)} %bitcast.15, bf16[128,2048]{1,0:T(8,128)(2,1)} %bitcast.20, ...), custom_call_target="tpu_custom_call" | custom-call | tf_op jit(solution)/shard_map/pallas_call | solution.py:606
  15.4 1.3 %shard_map.92 = bf16[384,2048]{1,0:T(8,128)(2,1)} custom-call(bf16[768,1024]{1,0:T(8,128)(2,1)S(1)} %get-tuple-element.9.act, bf16[1024,2048]{1,0:T(8,128)(2,1)S(1)} %get-tuple-element.10.wout, bf16[384,1536]{1,0:T(8,128)(2,1)S(1)} %get-tuple-element.11.out_left, bf16[1,384,512]{2,1,0:T(8,128)(2,1)S(1)} %get-tuple-element.12.landing_right), custom_call_target="tpu_custom_call" | custom-call | tf_op jit(solution)/shard_map/pallas_call | solution.py:656

commit v5 on v4

--- a/solution.py
+++ b/solution.py
@@ -14,7 +14,8 @@
 CHUNK = 256
 COLS = 512
 PAIR = 2
-LEAD_PARTS = 2
+LEAD_PARTS = 4
+FINAL_PARTS = 2
 F32 = jnp.float32
 BF16 = jnp.bfloat16
 scope = jax.named_scope
@@ -560,18 +561,28 @@
     left = pltpu.make_async_copy(out_left, out.at[:, pl.ds(0, left_width)], sem.at[0])
     left.start()
 
-    def right(t):
+    piece = half_rows // FINAL_PARTS
+
+    def right(t, k):
+        rows_at = pl.ds(k * piece, piece)
         at = pl.ds(left_width + t * COLS, COLS)
-        return pltpu.make_async_copy(out_right.at[t], out.at[:, at], sem.at[1 + t])
-
-    mine = act[pl.ds(pl.multiple_of(me_tp * half_rows, half_rows), half_rows), :]
+        return pltpu.make_async_copy(
+            out_right.at[t, rows_at, :], out.at[rows_at, at], sem.at[1 + t * FINAL_PARTS + k]
+        )
+
     for t in range(right_tiles):
         at = pl.ds(left_width + t * COLS, COLS)
-        out_right[t] = (dot(mine, wout[:, at]) + landing_right[t].astype(F32)).astype(BF16)
-        right(t).start()
+        for k in range(FINAL_PARTS):
+            rows_at = pl.ds(k * piece, piece)
+            mine = act[pl.ds(pl.multiple_of(me_tp * half_rows + k * piece, piece), piece), :]
+            out_right[t, rows_at, :] = (
+                dot(mine, wout[:, at]) + landing_right[t, rows_at, :].astype(F32)
+            ).astype(BF16)
+            right(t, k).start()
     left.wait()
     for t in range(right_tiles):
-        right(t).wait()
+        for k in range(FINAL_PARTS):
+            right(t, k).wait()
 
 
 def shards(n_sp, tokens, gain, wq, wk, wv, sink, wp, wo, wpo):
@@ -660,7 +671,7 @@
         out_specs=hbm,
         scratch_shapes=[
             pltpu.VMEM((tiles - left_tiles, half_rows, COLS), BF16),
-            dma((1 + tiles - left_tiles,)),
+            dma((1 + (tiles - left_tiles) * FINAL_PARTS,)),
         ],
         compiler_params=pltpu.CompilerParams(vmem_limit_bytes=spare // 3),
     )(act, wout, out_left, landing_right)

time: 16.9 us -> 16.9 us (level)
  no operation moved by 1% of the time
where the time goes in v5:
time: 16.9 us; the launch traced here: 16.7 us
  Pallas kernels  16.7 us (99%)
    pallas_call x1, Pallas kernels, shards(): pl.pallas_call(functools.partial(mix_kernel, n_sp, heads, local_kv, head_...  15.4 us
    pallas_call x1, Pallas kernels, shards(): pl.pallas_call(finish_kernel, out_shape=jax.ShapeDtypeStruct((half_rows,...  1.3 us

profile of v5, /device:TPU:0, one launch (start us, length us, event | category | flops | bytes accessed | tf_op | source)
XLA Modules:
  0.0 16.7 jit_solution(3146175457164873861)
XLA Ops:
  0.0 15.4 %shard_map.91 = (bf16[768,1024]{1,0:T(8,128)(2,1)S(1)}, bf16[384,1536]{1,0:T(8,128)(2,1)S(1)}, bf16[1,384,512]{2,1,0:T(8,128)(2,1)S(1)}, bf16[1024,2048]{1,0:T(8,128)(2,1)S(1)}) custom-call(bf16[768,1024]{1,0:T(8,128)(2,1)} %bitcast.19, f32[1,2048]{1,0:T(1,128)} %bitcast.22, bf16[512,2048]{1,0:T(8,128)(2,1)} %bitcast.15, bf16[128,2048]{1,0:T(8,128)(2,1)} %bitcast.20, ...), custom_call_target="tpu_custom_call" | custom-call | tf_op jit(solution)/shard_map/pallas_call | solution.py:617
  15.4 1.3 %shard_map.92 = bf16[384,2048]{1,0:T(8,128)(2,1)} custom-call(bf16[768,1024]{1,0:T(8,128)(2,1)S(1)} %get-tuple-element.9.act, bf16[1024,2048]{1,0:T(8,128)(2,1)S(1)} %get-tuple-element.10.wout, bf16[384,1536]{1,0:T(8,128)(2,1)S(1)} %get-tuple-element.11.out_left, bf16[1,384,512]{2,1,0:T(8,128)(2,1)S(1)} %get-tuple-element.12.landing_right), custom_call_target="tpu_custom_call" | custom-call | tf_op jit(solution)/shard_map/pallas_call | solution.py:667
